TPU v7x, 32 devices: a whole 2x2x4 slice. The times are simulated.
32 devices in a mesh: grp: 2 (over y), sp: 4 (over z), tp: 4 (over x, core).
Axes of the slice: x: 2, y: 2, z: 4, core: 2. Of those that a mesh axis runs over, the one named last changes fastest.
Arguments:
- tokens: bfloat16 [4096, 2048], P(('grp', 'sp', 'tp')), parts along dimension 0, may hold values from -6 to 6
- norm_gain: bfloat16 [2048], replicated, may hold values from 0.099609375 to 1.8984375
- conv_outer_weight: bfloat16 [2048, 1024], P('sp', 'tp'), may hold values from -0.125 to 0.125
- conv_inner_weight: bfloat16 [2048, 1024], P('sp', 'tp'), may hold values from -0.125 to 0.125
- conv_input_weight: bfloat16 [2048, 1024], P('sp', 'tp'), may hold values from -0.125 to 0.125
- query_matrix: bfloat16 [2048, 1024], P('sp', 'tp'), may hold values from -0.125 to 0.125
- key_weight: bfloat16 [2048, 1024], P('sp', 'tp'), may hold values from -0.125 to 0.125
- value_weight: bfloat16 [2048, 1024], P('sp', 'tp'), may hold values from -0.125 to 0.125
- gate_weight: bfloat16 [2048, 1024], P('sp', 'tp'), may hold values from -0.125 to 0.125
- conv_taps: bfloat16 [3, 1024], P(None, 'tp'), may hold values from -3.5 to 3.5
- conv_out_weight: bfloat16 [1024, 2048], P('tp', 'sp'), may hold values from -0.125 to 0.125
- ret_out_weight: bfloat16 [1024, 2048], P('tp', 'sp'), may hold values from -0.125 to 0.125
- log_decay: float32 [4096, 8], P(('grp', 'sp'), 'tp'), parts along dimension 0, may hold values from -0.75 to 0
Outputs:
- mixed: bfloat16 [4096, 2048], P(('grp', 'sp', 'tp')), parts along dimension 0
There are 2 independent parts, one for each index of `grp`. A program takes and returns all parts, laid end to end along the dimension named above; an argument that names none is the same for every part. Nothing has to cross between parts.
All inputs are finite; a program needn't handle non-finite values.
Results may differ from a plain program's by a relative error of at most 0.025.
Values may be sent and summed in bfloat16 or wider, within the bound.
A program may use at most 64 MiB of HBM per device.

v0:
```python
import jax
import jax.numpy as jnp
from jax import lax
from jax.sharding import PartitionSpec as P

HEAD = 128
CONV_K = 3
BLOCK = 128


EPSILON = 1e-06
ROTARY_BASE = 10000.0
HIGHEST_PRECISION = lax.Precision.HIGHEST


def prefix_2(x, axis, join, neutral):
    place = lax.axis_index(axis)
    gathered = jax.tree.map(
        lambda a, kind: lax.all_gather(a.astype(kind), axis), x, (jnp.bfloat16, jnp.bfloat16)
    )
    state = jax.tree.map(lambda a, e: jnp.zeros_like(a) + jnp.asarray(e, a.dtype), x, neutral)

    def one(turn, state):
        return join(
            state,
            jax.tree.map(
                lambda a, own: lax.dynamic_index_in_dim(a, turn, 0, False).astype(own.dtype),
                gathered,
                x,
            ),
        )

    return lax.fori_loop(0, place, one, state)


def shifted(x, axis, by):
    count = lax.axis_size(axis)
    pairs = [(i, i + by) for i in range(count) if 0 <= i + by < count]
    return lax.ppermute(x, axis, pairs)


def rotate(head_data, positions):
    half_width = head_data.shape[-1] // 2
    inv_freq = ROTARY_BASE ** (-jnp.arange(half_width, dtype=jnp.float32) / half_width)
    angles = positions[:, None] * inv_freq[None, :]
    cosine = jnp.cos(angles)[:, None, :]
    sine_part = jnp.sin(angles)[:, None, :]
    first_half = head_data[..., :half_width]
    second_half = head_data[..., half_width:]
    return jnp.concatenate(
        [
            first_half * cosine - second_half * sine_part,
            second_half * cosine + first_half * sine_part,
        ],
        axis=-1,
    )


def head_norm(head_data):
    return head_data * lax.rsqrt(jnp.mean(head_data * head_data, axis=-1, keepdims=True) + EPSILON)


def combine_states(earlier, later):
    return (earlier[0] * later[0], later[0][:, None, None] * earlier[1] + later[1])


def body(
    tokens,
    norm_gain,
    conv_outer_weight,
    conv_inner_weight,
    conv_input_weight,
    query_matrix,
    key_weight,
    value_weight,
    gate_weight,
    conv_taps,
    conv_out_weight,
    ret_out_weight,
    log_decay,
):
    values32 = tokens.astype(jnp.float32)
    normed = (
        values32
        * lax.rsqrt(jnp.mean(values32 * values32, axis=-1, keepdims=True) + EPSILON)
        * norm_gain.astype(jnp.float32)
    ).astype(jnp.bfloat16)
    gathered = lax.all_gather(normed, "tp", axis=0, tiled=True)
    row_total = gathered.shape[0]
    whole = (
        lax.all_gather(conv_outer_weight, "sp", axis=0, tiled=True),
        lax.all_gather(conv_inner_weight, "sp", axis=0, tiled=True),
        lax.all_gather(conv_input_weight, "sp", axis=0, tiled=True),
        lax.all_gather(query_matrix, "sp", axis=0, tiled=True),
        lax.all_gather(key_weight, "sp", axis=0, tiled=True),
        lax.all_gather(value_weight, "sp", axis=0, tiled=True),
        lax.all_gather(gate_weight, "sp", axis=0, tiled=True),
    )
    projected = tuple(
        (
            jnp.dot(gathered, weight, preferred_element_type=jnp.float32).astype(jnp.bfloat16)
            for weight in whole
        )
    )
    conv_outer, conv_inner, conv_input, query_proj, key_proj, value_proj, gate_proj = projected
    heads_here = query_proj.shape[1] // HEAD
    offset = (lax.axis_index("sp") * row_total).astype(jnp.float32)
    positions = offset + jnp.arange(row_total, dtype=jnp.float32)
    head_shape = (row_total, heads_here, HEAD)
    queries = rotate(query_proj.astype(jnp.float32).reshape(head_shape), positions)
    keys_rot = rotate(key_proj.astype(jnp.float32).reshape(head_shape), positions) * HEAD ** (-0.5)
    head_values = value_proj.astype(jnp.float32).reshape(head_shape)
    block_count = row_total // BLOCK
    block_shape = (block_count, BLOCK, heads_here, HEAD)
    query_blocks = queries.reshape(block_shape)
    key_blocks = keys_rot.reshape(block_shape)
    value_blocks = head_values.reshape(block_shape)
    log_blocks = log_decay.reshape(block_count, BLOCK, heads_here)
    offsets = jnp.arange(BLOCK, dtype=jnp.int32)
    causal_mask = offsets[:, None] >= offsets[None, :]
    lower_ones = causal_mask.astype(jnp.float32)
    cumulative = jnp.einsum("ij,njh->nih", lower_ones, log_blocks, precision=HIGHEST_PRECISION)
    block_end = cumulative[:, -1, :]
    mixed_in = conv_inner.astype(jnp.float32) * conv_input.astype(jnp.float32)
    rim = shifted(mixed_in[row_total - (CONV_K - 1) :], "sp", 1)
    extended = jnp.concatenate([rim, mixed_in], axis=0)
    taps = conv_taps.astype(jnp.float32)
    conv_out = jnp.zeros(mixed_in.shape, jnp.float32)
    for tap_index in range(CONV_K):
        conv_out = conv_out + taps[tap_index][None, :] * extended[tap_index : tap_index + row_total]
    conv_branch = (conv_outer.astype(jnp.float32) * conv_out).astype(jnp.bfloat16)
    weights = jnp.exp(block_end[:, None, :] - cumulative)
    increments = jnp.einsum(
        "njh,njhd,njhe->nhde", weights, key_blocks, value_blocks, precision=HIGHEST_PRECISION
    )

    def carry_on(carried, pieces):
        block_decay, increment = pieces
        return (block_decay[:, None, None] * carried + increment, carried)

    start_state = jnp.zeros((heads_here, HEAD, HEAD), jnp.float32)
    local_end, local_before = lax.scan(carry_on, start_state, (jnp.exp(block_end), increments))
    device_decay = jnp.exp(jnp.sum(block_end, axis=0))
    incoming = prefix_2(
        (device_decay, local_end),
        "sp",
        combine_states,
        (jnp.ones_like(device_decay), jnp.zeros_like(local_end)),
    )
    local_before, incoming_state = (local_before, incoming[1])
    spread = cumulative[:, :, None, :] - cumulative[:, None, :, :]
    grid_mask = causal_mask[None, :, :, None]
    decay_grid = jnp.where(grid_mask, jnp.exp(jnp.where(grid_mask, spread, 0.0)), 0.0)
    scores = (
        jnp.einsum("nihd,njhd->nijh", query_blocks, key_blocks, precision=HIGHEST_PRECISION)
        * decay_grid
    )
    within = jnp.einsum("nijh,njhe->nihe", scores, value_blocks, precision=HIGHEST_PRECISION)
    prefix = jnp.exp(jnp.cumsum(block_end, axis=0) - block_end)
    before = local_before + prefix[:, :, None, None] * incoming_state[None]
    across = jnp.einsum("nihd,nhde->nihe", query_blocks, before, precision=HIGHEST_PRECISION)
    across = across * jnp.exp(cumulative)[..., None]
    retained = (within + across).reshape(head_shape)
    ret_branch = (
        head_norm(retained).reshape(row_total, heads_here * HEAD)
        * jax.nn.silu(gate_proj.astype(jnp.float32))
    ).astype(jnp.bfloat16)
    conv_rows_weight, ret_rows_weight = (
        lax.all_gather(conv_out_weight, "sp", axis=1, tiled=True),
        lax.all_gather(ret_out_weight, "sp", axis=1, tiled=True),
    )
    return lax.psum_scatter(
        (
            jnp.dot(conv_branch, conv_rows_weight, preferred_element_type=jnp.float32)
            + jnp.dot(ret_branch, ret_rows_weight, preferred_element_type=jnp.float32)
        ).astype(jnp.bfloat16),
        "tp",
        scatter_dimension=0,
        tiled=True,
    )


def solution(mesh):
    placed = (
        P(("grp", "sp", "tp"), None),
        P(),
        P("sp", "tp"),
        P("sp", "tp"),
        P("sp", "tp"),
        P("sp", "tp"),
        P("sp", "tp"),
        P("sp", "tp"),
        P("sp", "tp"),
        P(None, "tp"),
        P("tp", "sp"),
        P("tp", "sp"),
        P(("grp", "sp"), "tp"),
    )
    return jax.shard_map(
        body, mesh=mesh, in_specs=placed, out_specs=P(("grp", "sp", "tp"), None), check_vma=False
    )
```

profile of v0, /device:TPU:11, one launch (start us, length us, event | category | flops | bytes accessed | tf_op | source)
XLA Modules:
  0.0 341.2 jit_solution(5092971589011308150)
XLA Ops:
  6.5 0.7 all-gather.25.cloned.1.call-update
  7.3 0.7 convert_element_type.96
  8.0 1.3 fusion.9
  9.3 2.0 fusion.11
  11.4 0.7 all-gather.27.cloned.1.call-update
  13.9 0.7 all-gather.15.cloned.1.call-update
  14.6 0.7 all-gather.21.cloned.1.call-update
  15.4 0.7 all-gather.29.cloned.1.call-update
  20.9 7.7 %all-reduce = bf16[8]{0:T(256)(128)(2,1)S(1)} all-reduce(bf16[8]{0:T(256)(128)(2,1)S(1)} %dynamic-update-slice), channel_id=2, replica_groups=mesh['grp'=2,'sp'=4,'tp'=4] {'sp'}, use_global_device_ids=true, to_apply=%add | all-reduce | flops 8 | bytes 32
  31.1 1.8 multiply_cosine_fusion
  32.9 4.6 %all-gather.25.cloned.1.call-done = bf16[2048,256]{1,0:T(8,128)(2,1)} async-done(((bf16[512,256]{1,0:T(8,128)(2,1)}), bf16[2048,256]{1,0:T(8,128)(2,1)}) %all-gather.25.cloned.1.call-update) | async-done | bytes 1048592 | tf_op jit(solution)/shard_map/all_gather | solution.py:95
  37.5 23.9 %all-gather.13.cloned.1.call-done = bf16[512,2048]{1,0:T(8,128)(2,1)} async-done(((bf16[128,2048]{1,0:T(8,128)(2,1)}), bf16[512,2048]{1,0:T(8,128)(2,1)}) %all-gather.13.cloned.1.call-update) | async-done | bytes 2097168 | tf_op jit(solution)/shard_map/all_gather | solution.py:88
  61.4 2.6 convolution_convert_fusion.2
  64.1 1.0 copy.95
  65.1 1.0 copy.96
  66.1 24.6 %all-gather.27.cloned.1.call-done = bf16[2048,256]{1,0:T(8,128)(2,1)} async-done(((bf16[512,256]{1,0:T(8,128)(2,1)}), bf16[2048,256]{1,0:T(8,128)(2,1)}) %all-gather.27.cloned.1.call-update) | async-done | bytes 1048592 | tf_op jit(solution)/shard_map/all_gather | solution.py:94
  90.7 2.0 convolution_convert_fusion.1
  92.7 1.0 copy.97
  93.7 1.0 copy.98
  94.7 24.8 %all-gather.23.cloned.1.call-done = bf16[2048,256]{1,0:T(8,128)(2,1)} async-done(((bf16[512,256]{1,0:T(8,128)(2,1)}), bf16[2048,256]{1,0:T(8,128)(2,1)}) %all-gather.23.cloned.1.call-update) | async-done | bytes 1048592 | tf_op jit(solution)/shard_map/all_gather | solution.py:96
  119.5 1.9 convolution_convert_fusion.3
  121.5 2.9 multiply_subtract_fusion
  124.4 1.7 fusion.23
  126.0 9.4 %while.26 = (s32[]{:T(128)}, f32[2,128,128]{2,1,0:T(8,128)S(1)}, f32[4,2,128,128]{3,2,1,0:T(8,128)}, f32[4,2]{1,0:T(4,128)}, f32[4,2,128,128]{3,2,1,0:T(8,128)}, /*index=5*/s32[]{:T(128)}, s32[]{:T(128)}) while((s32[]{:T(128)}, f32[2,128,128]{2,1,0:T(8,128)S(1)}, f32[4,2,128,128]{3,2,1,0:T(8,128)}, f32[4,2]{1,0:T(4,128)}, ...), condition=%wide.region_2.3_spmd.clone, body=%wide.region_1.2_spmd.clone.sunk | while | flops 131075 | bytes 655992 | solution.py:142
  127.4 1.0 bitcast_add_fusion.2
  129.7 1.0 bitcast_add_fusion.2
  132.1 1.0 bitcast_add_fusion.2
  133.1 0.7 bitcast_dynamic-update-slice_fusion.2
  134.4 1.0 bitcast_add_fusion.2
  135.4 14.1 %all-gather.1 = bf16[8,128,128]{2,1,0:T(8,128)(2,1)} all-gather(bf16[2,128,128]{2,1,0:T(8,128)(2,1)S(1)} %convert_element_type.112), channel_id=3, replica_groups=mesh['grp'=2,'sp'=4,'tp'=4] {'sp'}, dimensions={0}, use_global_device_ids=true | all-gather | bytes 327680 | tf_op jit(solution)/shard_map/all_gather | solution.py:19
  149.6 1.6 while.25
  149.6 0.7 bitcast_convert_fusion.2
  150.3 0.9 convert_add_fusion.2
  151.2 1.1 all-gather.19.cloned.1.call-done
  152.4 2.7 fusion.7
  155.1 26.2 %all-gather.17.cloned.1.call-done = bf16[2048,256]{1,0:T(8,128)(2,1)} async-done(((bf16[512,256]{1,0:T(8,128)(2,1)}), bf16[2048,256]{1,0:T(8,128)(2,1)}) %all-gather.17.cloned.1.call-update) | async-done | bytes 1048592 | tf_op jit(solution)/shard_map/all_gather | solution.py:92
  181.3 2.2 fusion.6
  184.1 3.0 collective-permute-start
  187.5 1.3 fusion.3
  189.3 1.9 multiply_reduce_fusion
  191.3 1.3 copy.85
  192.7 17.6 %all-gather.15.cloned.1.call-done = bf16[2048,256]{1,0:T(8,128)(2,1)} async-done(((bf16[512,256]{1,0:T(8,128)(2,1)}), bf16[2048,256]{1,0:T(8,128)(2,1)}) %all-gather.15.cloned.1.call-update) | async-done | bytes 1048592 | tf_op jit(solution)/shard_map/all_gather | solution.py:91
  210.3 29.0 %all-gather.21.cloned.1.call-done = bf16[256,2048]{1,0:T(8,128)(2,1)} async-done(((bf16[256,512]{1,0:T(8,128)(2,1)}), bf16[256,2048]{1,0:T(8,128)(2,1)}) %all-gather.21.cloned.1.call-update) | async-done | bytes 1048592 | tf_op jit(solution)/shard_map/all_gather | solution.py:169
  239.3 5.8 %fusion.30 = f32[512,2048]{1,0:T(8,128)} fusion(bf16[256,2048]{1,0:T(8,128)(2,1)} %all-gather.21.cloned.1.call-done, f32[2,256]{1,0:T(2,128)} %collective-permute-done, f32[512,256]{1,0:T(8,128)S(1)} %copy-done.2, bf16[512,2048]{1,0:T(8,128)(2,1)S(1)} %copy-done, bf16[2048,256]{1,0:T(8,128)(2,1)} %all-gather.15.cloned.1.call-done, f32[256]{0:T(256)S(1)} %bitcast.101, ...), kind=kOutput, calls=%fused_computation.62 | convolution fusion | flops 1075183616 | bytes 8918016 | tf_op jit(solution)/shard_map/dot_general | solution.py:174
  245.1 23.1 %all-gather.29.cloned.1.call-done = bf16[2048,256]{1,0:T(8,128)(2,1)} async-done(((bf16[512,256]{1,0:T(8,128)(2,1)}), bf16[2048,256]{1,0:T(8,128)(2,1)}) %all-gather.29.cloned.1.call-update) | async-done | bytes 1048592 | tf_op jit(solution)/shard_map/all_gather | solution.py:97
  268.2 28.8 %all-gather.31.cloned.1.call-done = bf16[256,2048]{1,0:T(8,128)(2,1)} async-done(((bf16[256,512]{1,0:T(8,128)(2,1)}), bf16[256,2048]{1,0:T(8,128)(2,1)}) %all-gather.31.cloned.1.call-update) | async-done | bytes 1048592 | tf_op jit(solution)/shard_map/all_gather | solution.py:170
  297.6 6.5 %add_convert_fusion = bf16[512,2048]{1,0:T(8,128)(2,1)} fusion(f32[512,2048]{1,0:T(8,128)} %fusion.30, bf16[256,2048]{1,0:T(8,128)(2,1)} %all-gather.31.cloned.1.call-done, f32[64,8,2,128]{3,2,1,0:T(2,128)S(1)} %bitcast.95, f32[64,8,2,128]{3,2,1,0:T(2,128)S(1)} %bitcast.94, bf16[512,2048]{1,0:T(8,128)(2,1)S(1)} %copy-done, ...), kind=kOutput, calls=%fused_computation.6 | convolution fusion | flops 1077018624 | bytes 11534336 | tf_op jit(solution)/shard_map/dot_general | solution.py:175
  304.2 30.5 %reduce-scatter.2.cloned.1.call-done = bf16[128,2048]{1,0:T(8,128)(2,1)} async-done(((bf16[512,2048]{1,0:T(8,128)(2,1)}), bf16[128,2048]{1,0:T(8,128)(2,1)}) %reduce-scatter.2.cloned.1.call-update) | async-done | bytes 524304 | tf_op jit(solution)/shard_map/reduce_scatter | solution.py:172
  (92 shorter events, 15.5 us)
Async XLA Ops:
  6.5 30.9 %all-gather.25.cloned.1.call-start = ((), (), s32[]{:S(2)}) async-start(), calls=%async_computation.7 | async-start | bytes 1310720 | tf_op jit(solution)/shard_map/all_gather | solution.py:95
  7.3 54.1 %all-gather.13.cloned.1.call-start = ((), (), s32[]{:S(2)}) async-start(), calls=%async_computation.1 | async-start | bytes 2621440 | tf_op jit(solution)/shard_map/all_gather | solution.py:88
  8.0 8.7 %copy-start.14 = (f32[512,2]{0,1:T(2,128)S(1)}, f32[512,2]{0,1:T(2,128)}, u32[]{:S(2)}) copy-start(f32[512,2]{0,1:T(2,128)} %param.29) | copy-start | bytes 12292
  8.0 10.7 %copy-start.15 = (u32[32]{0:T(128)S(1)}, u32[32]{0:T(128)}, u32[]{:S(2)}) copy-start(u32[32]{0:T(128)} %constant.65) | copy-start | bytes 388
  8.0 22.5 %copy-start.10 = (bf16[3,256]{1,0:T(4,128)(2,1)S(1)}, bf16[3,256]{1,0:T(4,128)(2,1)}, u32[]{:S(2)}) copy-start(bf16[3,256]{1,0:T(4,128)(2,1)} %param.26) | copy-start | bytes 4612
  11.3 79.3 %all-gather.27.cloned.1.call-start = ((), (), s32[]{:S(2)}) async-start(), calls=%async_computation.8 | async-start | bytes 1310720 | tf_op jit(solution)/shard_map/all_gather | solution.py:94
  12.1 107.4 %all-gather.23.cloned.1.call-start = ((), (), s32[]{:S(2)}) async-start(), calls=%async_computation.6 | async-start | bytes 1310720 | tf_op jit(solution)/shard_map/all_gather | solution.py:96
  12.6 139.7 %all-gather.19.cloned.1.call-start = ((), (), s32[]{:S(2)}) async-start(), calls=%async_computation.4 | async-start | bytes 1310720 | tf_op jit(solution)/shard_map/all_gather | solution.py:93
  13.2 168.1 %all-gather.17.cloned.1.call-start = ((), (), s32[]{:S(2)}) async-start(), calls=%async_computation.3 | async-start | bytes 1310720 | tf_op jit(solution)/shard_map/all_gather | solution.py:92
  13.8 196.5 %all-gather.15.cloned.1.call-start = ((), (), s32[]{:S(2)}) async-start(), calls=%async_computation.2 | async-start | bytes 1310720 | tf_op jit(solution)/shard_map/all_gather | solution.py:91
  14.6 224.7 %all-gather.21.cloned.1.call-start = ((), (), s32[]{:S(2)}) async-start(), calls=%async_computation.5 | async-start | bytes 1310720 | tf_op jit(solution)/shard_map/all_gather | solution.py:169
  15.3 252.9 %all-gather.29.cloned.1.call-start = ((), (), s32[]{:S(2)}) async-start(), calls=%async_computation.9 | async-start | bytes 1310720 | tf_op jit(solution)/shard_map/all_gather | solution.py:97
  16.0 281.0 %all-gather.31.cloned.1.call-start = ((), (), s32[]{:S(2)}) async-start(), calls=%async_computation.10 | async-start | bytes 1310720 | tf_op jit(solution)/shard_map/all_gather | solution.py:170
  16.6 318.0 %reduce-scatter.2.cloned.1.call-start = ((), (), s32[]{:S(2)}) async-start(), calls=%async_computation.11 | async-start | bytes 2621440 | tf_op jit(solution)/shard_map/reduce_scatter | solution.py:172
  64.0 26.7 %copy-start = (bf16[512,2048]{1,0:T(8,128)(2,1)S(1)}, bf16[512,2048]{1,0:T(8,128)(2,1)}, u32[]{:S(2)}) copy-start(bf16[512,2048]{1,0:T(8,128)(2,1)} %all-gather.13.cloned.1.call-done) | copy-start | bytes 6291460
  121.5 2.9 copy-start.8
  181.3 5.9 %copy-start.3 = (f32[512,2,64]{2,0,1:T(8,128)S(1)}, f32[512,2,64]{2,0,1:T(8,128)}, u32[]{:S(2)}) copy-start(f32[512,2,64]{2,0,1:T(8,128)} %get-tuple-element.140) | copy-start | bytes 786436
  181.3 5.9 %copy-start.4 = (f32[512,2,64]{2,0,1:T(8,128)S(1)}, f32[512,2,64]{2,0,1:T(8,128)}, u32[]{:S(2)}) copy-start(f32[512,2,64]{2,0,1:T(8,128)} %get-tuple-element.141) | copy-start | bytes 786436
  181.3 6.1 %copy-start.6 = (f32[4,128,2]{1,2,0:T(2,128)S(1)}, f32[4,128,2]{1,2,0:T(2,128)}, u32[]{:S(2)}) copy-start(f32[4,128,2]{1,2,0:T(2,128)} %copy.73) | copy-start | bytes 12292
  183.5 3.7 %copy-start.1 = (f32[512,256]{1,0:T(8,128)}, f32[512,256]{1,0:T(8,128)S(1)}, u32[]{:S(2)}) copy-start(f32[512,256]{1,0:T(8,128)S(1)} %fusion.6) | copy-start | bytes 1572868
  184.1 55.1 %collective-permute-start = (f32[2,256]{1,0:T(2,128)}, f32[2,256]{1,0:T(2,128)}, u32[]{:S(2)}, u32[]{:S(2)}) collective-permute-start(f32[2,256]{1,0:T(2,128)} %slice.45), channel_id=1, source_target_pairs={{0,4},{4,8},{8,12},{1,5},{5,9},{9,13},{2,6},{6,10},{10,14},{3,7},{... | collective-permute-start | bytes 6152 | tf_op jit(solution)/shard_map/ppermute | solution.py:39
  187.4 1.8 copy-start.5
  187.4 1.8 copy-start.7
  187.4 1.8 copy-start.9
  189.2 50.0 %copy-start.2 = (f32[512,256]{1,0:T(8,128)S(1)}, f32[512,256]{1,0:T(8,128)}, u32[]{:S(2)}) copy-start(f32[512,256]{1,0:T(8,128)} %copy-done.1) | copy-start | bytes 1572868
  189.2 50.0 %copy-start.11 = (f32[1,256]{1,0:T(1,128)S(1)}, f32[1,256]{1,0:T(1,128)}, u32[]{:S(2)}) copy-start(f32[1,256]{1,0:T(1,128)} %get-tuple-element.154) | copy-start | bytes 3076
  189.2 50.0 %copy-start.12 = (f32[1,256]{1,0:T(1,128)S(1)}, f32[1,256]{1,0:T(1,128)}, u32[]{:S(2)}) copy-start(f32[1,256]{1,0:T(1,128)} %get-tuple-element.155) | copy-start | bytes 3076
  189.2 50.0 %copy-start.13 = (f32[1,256]{1,0:T(1,128)S(1)}, f32[1,256]{1,0:T(1,128)}, u32[]{:S(2)}) copy-start(f32[1,256]{1,0:T(1,128)} %get-tuple-element.156) | copy-start | bytes 3076
Sparse Core Ops, SparseCore 0:
  8.9 28.5 all-gather.24
  39.0 22.3 all-gather.12
  63.0 27.6 all-gather.26
  92.1 27.3 all-gather.22
  120.9 31.4 all-gather.18
  153.8 27.4 all-gather.16
  182.9 27.3 all-gather.14
  211.8 27.3 all-gather.20
  240.8 27.3 all-gather.28
  269.6 27.3 all-gather.30
  304.3 30.2 reduce-scatter.1
where the time goes:
time: 345 us; the launch traced here: 341 us
  waiting for transfers between devices  240 us (70%)
  matrix products  29.2 us (8%)
  blocking collectives  21.9 us (6%)
  other arithmetic  17.6 us (5%)
  local copies, waits for them, and re-layouts  15.1 us (4%)
  between operations  14.2 us (4%)
    reduce_scatter x1, waiting for transfers between devices, body(): lax.psum_scatter((jnp.dot(conv_branch, conv_rows_weight, preferred_elemen...  30.5 us
    all_gather x1, waiting for transfers between devices, body(): lax.all_gather(conv_out_weight, 'sp', axis=1, tiled=True)  29 us
    all_gather x1, waiting for transfers between devices, body(): lax.all_gather(ret_out_weight, 'sp', axis=1, tiled=True)  28.8 us
    all_gather x1, waiting for transfers between devices, body(): lax.all_gather(conv_inner_weight, 'sp', axis=0, tiled=True)  26.2 us
    all_gather x1, waiting for transfers between devices, body(): lax.all_gather(value_weight, 'sp', axis=0, tiled=True)  24.8 us
    all_gather x1, waiting for transfers between devices, body(): lax.all_gather(query_matrix, 'sp', axis=0, tiled=True)  24.6 us
    all_gather x1, waiting for transfers between devices, body(): gathered = lax.all_gather(normed, 'tp', axis=0, tiled=True)  23.9 us
    all_gather x1, waiting for transfers between devices, body(): lax.all_gather(gate_weight, 'sp', axis=0, tiled=True)  23.1 us
  transfers between devices with their start and end apart: 12, of which 11 were waited for; matrix products, arithmetic and copies ran while one was open for 16% of the time, Pallas kernels for 0%

commit v1 on v0

--- a/solution.py
+++ b/solution.py
@@ -1,6 +1,10 @@
+import functools
+
 import jax
 import jax.numpy as jnp
 from jax import lax
+from jax.experimental import pallas as pl
+from jax.experimental.pallas import tpu as pltpu
 from jax.sharding import PartitionSpec as P
 
 HEAD = 128
@@ -180,6 +184,402 @@
     )
 
 
+MESH = pl.DeviceIdType.MESH
+NPROJ = 7
+LAG = 2
+ORDER = (3, 4, 5, 6, 0, 1, 2)
+QUERY, KEY, VALUE, GATE, OUTER, INNER, INPUT = range(NPROJ)
+
+
+def remote(src, dst, send, recv, axis, to):
+    return pltpu.make_async_remote_copy(
+        src_ref=src, dst_ref=dst, send_sem=send, recv_sem=recv, device_id={axis: to}, device_id_type=MESH
+    )
+
+
+def kernel(sizes, *refs):
+    n, g, m = sizes
+    tokens, gain, w0, w1, w2, w3, w4, w5, w6, taps, oc, orr, ld, ldt, cos2, sin2, out = refs[:17]
+    (raw, xn, gw, go, acc, ext, qr, kr, cum_s, cumt_s, lend, dec, instate, indec, sin_s, rb, cb, stage, land, tail, own) = refs[17:38]
+    (tsend, trecv, rsend, lsend, zrecv, ysend, yrecv, ssend, srecv, dsend, drecv, csend, crecv, osend, orecv) = refs[38:]
+    weights = [(w0, w1, w2, w3, w4, w5, w6)[i] for i in ORDER]
+    outs = (oc, orr)
+    me = lax.axis_index("sp")
+    grp = lax.axis_index("grp")
+    mine = lax.axis_index("tp")
+    rows, width = tokens.shape
+    total = rows * m
+    depth, cols = w0.shape
+    half = depth // 2
+    orows = oc.shape[0]
+    ohalf = orows // 2
+    ocols = oc.shape[1]
+    heads = cols // HEAD
+    other = 1 - grp
+
+    barrier = pltpu.get_barrier_semaphore()
+    for axis, count, at in (("sp", n, me), ("grp", g, grp), ("tp", m, mine)):
+        for d in range(1, count):
+            pl.semaphore_signal(barrier, inc=1, device_id={axis: lax.rem(at + d, count)}, device_id_type=MESH)
+    pl.semaphore_wait(barrier, n + g + m - 3)
+
+    def token_copy(d):
+        to = lax.rem(mine + d, m)
+        return remote(tokens, raw.at[d - 1], tsend.at[d - 1], trecv.at[d - 1], "tp", to)
+
+    for d in range(1, m):
+        token_copy(d).start()
+
+    hs = pl.ds(pl.multiple_of(grp * half, half), half)
+    ohs = pl.ds(pl.multiple_of(grp * ohalf, ohalf), ohalf)
+
+    def slot(w, s, is_out):
+        return go.at[w, s, ohs] if is_out else gw.at[w, s, hs]
+
+    def sem_at(w, is_out):
+        return w + NPROJ if is_out else w
+
+    def line_copy(w, s, is_out, right, src=None):
+        dst = slot(w, s, is_out)
+        k = sem_at(w, is_out)
+        to = me + 1 if right else me - 1
+        return remote(
+            dst if src is None else src, dst, (rsend if right else lsend).at[k, s], zrecv.at[k, s], "sp", to
+        )
+
+    def pair_copy(w, s, is_out):
+        part = slot(w, s, is_out)
+        k = sem_at(w, is_out)
+        return remote(part, part, ysend.at[k, s], yrecv.at[k, s], "grp", other)
+
+    for w, is_out in [(0, True), (1, True)] + [(w, False) for w in range(NPROJ)]:
+        src = outs[w].at[ohs] if is_out else weights[w].at[hs]
+
+        @pl.when(me < n - 1)
+        def _():
+            line_copy(w, me, is_out, True, src).start()
+
+        @pl.when(me > 0)
+        def _():
+            line_copy(w, me, is_out, False, src).start()
+
+    below = lax.broadcasted_iota(jnp.int32, (total, total), 0) >= lax.broadcasted_iota(jnp.int32, (total, total), 1)
+    cum_s[...] = jnp.dot(below.astype(jnp.float32), ld[...], precision=HIGHEST_PRECISION, preferred_element_type=jnp.float32)
+    above = lax.broadcasted_iota(jnp.int32, (total, total), 0) <= lax.broadcasted_iota(jnp.int32, (total, total), 1)
+    cumt_s[...] = jnp.dot(ldt[...], above.astype(jnp.float32), precision=HIGHEST_PRECISION, preferred_element_type=jnp.float32)
+
+    step_rows = 16
+    scale = gain[...].astype(jnp.float32)
+
+    def normalise(source, block):
+        def one(i, carry):
+            at = pl.multiple_of(i * step_rows, step_rows)
+            v = source[pl.ds(at, step_rows), :].astype(jnp.float32)
+            r = lax.rsqrt(jnp.mean(v * v, axis=-1, keepdims=True) + EPSILON)
+            y = (v * r * scale).astype(jnp.bfloat16)
+            to = pl.ds(pl.multiple_of(block * rows + at, step_rows), step_rows)
+            for s in range(n):
+                xn[s, to, :] = y[:, s * depth : (s + 1) * depth]
+            return carry
+
+        lax.fori_loop(0, rows // step_rows, one, 0)
+
+    normalise(tokens, mine)
+    for d in range(1, m):
+        token_copy(d).wait_recv()
+        normalise(raw.at[d - 1], lax.rem(mine - d + m, m))
+
+    for w in range(NPROJ):
+        acc[w] = jnp.dot(xn[me], weights[w][...], preferred_element_type=jnp.float32)
+    for w in range(2):
+        go[w, me] = outs[w][...]
+
+    def forward(w, is_out, d):
+        @pl.when(me >= d)
+        def _():
+            s = me - d
+            line_copy(w, s, is_out, True).wait_recv()
+
+            @pl.when(me < n - 1)
+            def _():
+                line_copy(w, s, is_out, True).start()
+
+            pair_copy(w, s, is_out).start()
+
+        @pl.when(me + d < n)
+        def _():
+            s = me + d
+            line_copy(w, s, is_out, False).wait_recv()
+
+            @pl.when(me > 0)
+            def _():
+                line_copy(w, s, is_out, False).start()
+
+            pair_copy(w, s, is_out).start()
+
+    def other_wait(w, s, is_out):
+        theirs = (
+            go.at[w, s, pl.ds(pl.multiple_of(other * ohalf, ohalf), ohalf)]
+            if is_out
+            else gw.at[w, s, pl.ds(pl.multiple_of(other * half, half), half)]
+        )
+        k = sem_at(w, is_out)
+        remote(theirs, theirs, ysend.at[k, s], yrecv.at[k, s], "grp", other).wait_recv()
+
+    def consume(w, d):
+        @pl.when(me >= d)
+        def _():
+            s = me - d
+            other_wait(w, s, False)
+            acc[w] += jnp.dot(xn[s], gw[w, s], preferred_element_type=jnp.float32)
+
+        @pl.when(me + d < n)
+        def _():
+            s = me + d
+            other_wait(w, s, False)
+            acc[w] += jnp.dot(xn[s], gw[w, s], preferred_element_type=jnp.float32)
+
+    def phase(d, lo, hi):
+        def one(i, carry):
+            @pl.when(i < hi)
+            def _():
+                forward(i, False, d)
+
+            @pl.when(i >= lo + LAG)
+            def _():
+                consume(i - LAG, d)
+
+            return carry
+
+        lax.fori_loop(lo, hi + LAG, one, 0)
+
+    for d in range(1, n):
+        forward(0, True, d)
+        forward(1, True, d)
+        if d < n - 1:
+            phase(d, 0, NPROJ)
+    phase(n - 1, 0, 3)
+
+    def projected(w, h=None):
+        part = acc[w] if h is None else acc[w, :, h * HEAD : (h + 1) * HEAD]
+        return part.astype(jnp.bfloat16).astype(jnp.float32)
+
+    def state_copy(d):
+        return remote(lend, instate.at[me], ssend.at[d - 1], srecv.at[me], "sp", me + d)
+
+    def decay_copy(d):
+        return remote(dec, indec.at[me], dsend.at[d - 1], drecv.at[me], "sp", me + d)
+
+    dec[...] = jnp.zeros_like(dec)
+    for h in range(heads):
+        k = projected(KEY, h)
+        k = (k * cos2[...] + pltpu.roll(k, HEAD // 2, 1) * sin2[...]) * HEAD ** (-0.5)
+        kr[h] = k.astype(jnp.bfloat16)
+        q = projected(QUERY, h)
+        qr[h] = (q * cos2[...] + pltpu.roll(q, HEAD // 2, 1) * sin2[...]).astype(jnp.bfloat16)
+        c = cum_s[:, h : h + 1]
+        end = cum_s[total - 1 : total, h : h + 1]
+        kw = (k * jnp.exp(end - c)).astype(jnp.bfloat16)
+        vals = acc[VALUE, :, h * HEAD : (h + 1) * HEAD].astype(jnp.bfloat16)
+        lend[h] = lax.dot_general(kw, vals, (((0,), (0,)), ((), ())), preferred_element_type=jnp.float32).astype(jnp.bfloat16)
+        dec[h : h + 1, :] = jnp.broadcast_to(end, (1, HEAD))
+    for d in range(1, n):
+
+        @pl.when(me + d < n)
+        def _():
+            state_copy(d).start()
+            decay_copy(d).start()
+
+    phase(n - 1, 3, NPROJ)
+
+    mixed_in = projected(INNER) * projected(INPUT)
+    ext[8:, :] = mixed_in
+    tail[...] = mixed_in[total - 8 :, :]
+
+    def rim_copy():
+        return remote(tail, ext.at[0:8], csend, crecv, "sp", me + 1)
+
+    @pl.when(me < n - 1)
+    def _():
+        rim_copy().start()
+
+    sin_s[...] = jnp.zeros_like(sin_s)
+    for s in range(n - 1):
+
+        @pl.when(me > s)
+        def _():
+            remote(lend, instate.at[s], ssend.at[0], srecv.at[s], "sp", s).wait_recv()
+            remote(dec, indec.at[s], dsend.at[0], drecv.at[s], "sp", s).wait_recv()
+            for h in range(heads):
+                sin_s[h] = jnp.exp(indec[s, h : h + 1, :]) * sin_s[h] + instate[s, h].astype(jnp.float32)
+
+    for h in range(heads):
+        c = cum_s[:, h : h + 1]
+        spread = c - cumt_s[h : h + 1, :]
+        grid = jnp.where(below, jnp.exp(jnp.where(below, spread, 0.0)), 0.0)
+        scores = lax.dot_general(qr[h], kr[h], (((1,), (1,)), ((), ())), preferred_element_type=jnp.float32) * grid
+        vals = acc[VALUE, :, h * HEAD : (h + 1) * HEAD].astype(jnp.bfloat16)
+        kept = jnp.dot(scores.astype(jnp.bfloat16), vals, preferred_element_type=jnp.float32)
+        kept += jnp.dot(qr[h], sin_s[h].astype(jnp.bfloat16), preferred_element_type=jnp.float32) * jnp.exp(c)
+        gate = projected(GATE, h)
+        normed = kept * lax.rsqrt(jnp.mean(kept * kept, axis=-1, keepdims=True) + EPSILON)
+        rb[:, h * HEAD : (h + 1) * HEAD] = (normed * (gate / (1.0 + jnp.exp(-gate)))).astype(jnp.bfloat16)
+
+    @pl.when(me > 0)
+    def _():
+        remote(tail, ext.at[0:8], csend, crecv, "sp", me - 1).wait_recv()
+
+    @pl.when(me == 0)
+    def _():
+        ext[0:8, :] = jnp.zeros((8, cols), jnp.float32)
+
+    t = taps[...].astype(jnp.float32)
+    conv = jnp.zeros((total, cols), jnp.float32)
+    for j in range(CONV_K):
+        lo = 8 - (CONV_K - 1) + j
+        conv = conv + t[j : j + 1, :] * ext[lo : lo + total, :]
+    cb[...] = (projected(OUTER) * conv).astype(jnp.bfloat16)
+
+    for d in range(1, n):
+        for w in range(2):
+
+            @pl.when(me >= d)
+            def _():
+                other_wait(w, me - d, True)
+
+            @pl.when(me + d < n)
+            def _():
+                other_wait(w, me + d, True)
+
+    def partial(block, s):
+        at = pl.ds(pl.multiple_of(block * rows, rows), rows)
+        return jnp.dot(cb[at, :], go[0, s], preferred_element_type=jnp.float32) + jnp.dot(
+            rb[at, :], go[1, s], preferred_element_type=jnp.float32
+        )
+
+    def out_copy(d):
+        return remote(stage.at[d - 1], land.at[d - 1], osend.at[d - 1], orecv.at[d - 1], "tp", lax.rem(mine + d, m))
+
+    for d in range(1, m):
+        block = lax.rem(mine + d, m)
+        for s in range(n):
+            stage[d - 1, :, s * ocols : (s + 1) * ocols] = partial(block, s).astype(jnp.bfloat16)
+        out_copy(d).start()
+    for s in range(n):
+        own[:, s * ocols : (s + 1) * ocols] = partial(mine, s)
+    for d in range(1, m):
+        out_copy(d).wait_recv()
+    for s in range(n):
+        at = slice(s * ocols, (s + 1) * ocols)
+        value = own[:, at].astype(jnp.bfloat16).astype(jnp.float32)
+        for d in range(1, m):
+            value = value + land[d - 1, :, at].astype(jnp.float32)
+        out[:, at] = value.astype(jnp.bfloat16)
+
+    for d in range(1, m):
+        token_copy(d).wait_send()
+        out_copy(d).wait_send()
+    for d in range(1, n):
+
+        @pl.when(me + d < n)
+        def _():
+            state_copy(d).wait_send()
+            decay_copy(d).wait_send()
+
+    @pl.when(me < n - 1)
+    def _():
+        rim_copy().wait_send()
+
+    for is_out, count in ((True, 2), (False, NPROJ)):
+
+        def drain(w, carry):
+            for s in range(n):
+
+                @pl.when((s <= me) & (me < n - 1))
+                def _():
+                    line_copy(w, s, is_out, True).wait_send()
+
+                @pl.when((s >= me) & (me > 0))
+                def _():
+                    line_copy(w, s, is_out, False).wait_send()
+
+                @pl.when(me != s)
+                def _():
+                    pair_copy(w, s, is_out).wait_send()
+
+            return carry
+
+        lax.fori_loop(0, count, drain, 0)
+
+
+def fused(sizes, *args):
+    n, g, m = sizes
+    tokens, gain, w0 = args[0], args[1], args[2]
+    log_decay = args[12]
+    rows, width = tokens.shape
+    depth, cols = w0.shape
+    orows, ocols = args[10].shape
+    total = rows * m
+    heads = cols // HEAD
+    half_width = HEAD // 2
+    inv_freq = ROTARY_BASE ** (-jnp.arange(half_width, dtype=jnp.float32) / half_width)
+    offset = (lax.axis_index("sp") * total).astype(jnp.float32)
+    angles = (offset + jnp.arange(total, dtype=jnp.float32))[:, None] * inv_freq[None, :]
+    cosine, sine = jnp.cos(angles), jnp.sin(angles)
+    cos2 = jnp.concatenate([cosine, cosine], axis=1)
+    sin2 = jnp.concatenate([-sine, sine], axis=1)
+    bf, f32 = jnp.bfloat16, jnp.float32
+    dma = pltpu.SemaphoreType.DMA
+    scratch = [
+        pltpu.VMEM((m - 1, rows, width), bf),
+        pltpu.VMEM((n, total, depth), bf),
+        pltpu.VMEM((NPROJ, n, depth, cols), bf),
+        pltpu.VMEM((2, n, orows, ocols), bf),
+        pltpu.VMEM((NPROJ, total, cols), f32),
+        pltpu.VMEM((total + 8, cols), f32),
+        pltpu.VMEM((heads, total, HEAD), bf),
+        pltpu.VMEM((heads, total, HEAD), bf),
+        pltpu.VMEM((total, heads), f32),
+        pltpu.VMEM((heads, total), f32),
+        pltpu.VMEM((heads, HEAD, HEAD), bf),
+        pltpu.VMEM((8, HEAD), f32),
+        pltpu.VMEM((n, heads, HEAD, HEAD), bf),
+        pltpu.VMEM((n, 8, HEAD), f32),
+        pltpu.VMEM((heads, HEAD, HEAD), f32),
+        pltpu.VMEM((total, cols), bf),
+        pltpu.VMEM((total, cols), bf),
+        pltpu.VMEM((m - 1, rows, width), bf),
+        pltpu.VMEM((m - 1, rows, width), bf),
+        pltpu.VMEM((8, cols), f32),
+        pltpu.VMEM((rows, width), f32),
+        dma((m - 1,)),
+        dma((m - 1,)),
+        dma((NPROJ + 2, n)),
+        dma((NPROJ + 2, n)),
+        dma((NPROJ + 2, n)),
+        dma((NPROJ + 2, n)),
+        dma((NPROJ + 2, n)),
+        dma((n,)),
+        dma((n,)),
+        dma((n,)),
+        dma((n,)),
+        dma,
+        dma,
+        dma((m - 1,)),
+        dma((m - 1,)),
+    ]
+    return pl.pallas_call(
+        functools.partial(kernel, sizes),
+        out_shape=jax.ShapeDtypeStruct((rows, width), bf),
+        in_specs=[pl.BlockSpec(memory_space=pltpu.VMEM)] * 16,
+        out_specs=pl.BlockSpec(memory_space=pltpu.VMEM),
+        scratch_shapes=scratch,
+        compiler_params=pltpu.CompilerParams(
+            collective_id=0, has_side_effects=True, vmem_limit_bytes=60 * 1024 * 1024
+        ),
+    )(tokens, gain[None, :], *args[2:12], log_decay, log_decay.T, cos2, sin2)
+
+
 def solution(mesh):
     placed = (
         P(("grp", "sp", "tp"), None),
@@ -196,6 +596,8 @@
         P("tp", "sp"),
         P(("grp", "sp"), "tp"),
     )
+    n, g, m = (mesh.shape[axis] for axis in ("sp", "grp", "tp"))
+    fits = g == 2 and 2 <= n <= 4
     return jax.shard_map(
-        body, mesh=mesh, in_specs=placed, out_specs=P(("grp", "sp", "tp"), None), check_vma=False
-    )
+        functools.partial(fused, (n, g, m)) if fits else body, mesh=mesh, in_specs=placed, out_specs=P(("grp", "sp", "tp"), None), check_vma=False
+    )

time: 345 us -> 136 us (0.39)
  waiting for transfers between devices: 240 us -> 0 us
  Pallas kernels: 0 us -> 130 us
  matrix products: 29.2 us -> 0 us
  blocking collectives: 21.9 us -> 0 us
  other arithmetic: 17.6 us -> 2 us
  between operations: 14.2 us -> 0.03 us
  local copies, waits for them, and re-layouts: 15.1 us -> 3.36 us
    all_gather x10 -> x0, waiting for transfers between devices: 204 us -> none  [the longest x1 29 us: body(): lax.all_gather(conv_out_weight, 'sp', axis=1, tiled=True)]
    pallas_call x0 -> x1, Pallas kernels: none -> 130 us  [fused(): pl.pallas_call(functools.partial(kernel, sizes), out_shape=jax.ShapeDtype...]
    reduce_scatter x1 -> x0, waiting for transfers between devices: 30.5 us -> none  [body(): lax.psum_scatter((jnp.dot(conv_branch, conv_rows_weight, preferred_elemen...]
    dot_general x12 -> x0, matrix products: 29.2 us -> none  [the longest x5 11.4 us: body(): jnp.dot(gathered, weight, preferred_element_type=jnp.float32)]
    all_gather x1 -> x0, blocking collectives: 14.1 us -> none  [prefix_2(): lax.all_gather(a.astype(kind), axis)]
    unnamed x1 -> x0, blocking collectives: 7.73 us -> none
    unnamed x11 -> x0, waiting for transfers between devices: 5.61 us -> none
    add x6 -> x1, other arithmetic: 4.88 us -> 0.01 us  [fused(): offset + jnp.arange(total, dtype=jnp.float32)]
  transfers between devices with their start and end apart: 12 -> 0, of which waited for: 11 -> 0; matrix products, arithmetic and copies ran while one was open for 16% -> 0% of each run, Pallas kernels for 0% -> 0%
where the time goes in v1:
time: 136 us; the launch traced here: 135 us
  Pallas kernels  130 us (96%)
  local copies, waits for them, and re-layouts  3.36 us (2%)
  other arithmetic  2 us (1%)
    pallas_call x1, Pallas kernels, fused(): pl.pallas_call(functools.partial(kernel, sizes), out_shape=jax.ShapeDtype...  130 us
    unnamed x6, local copies, waits for them, and re-layouts  2.75 us

profile of v1, /device:TPU:11, one launch (start us, length us, event | category | flops | bytes accessed | tf_op | source)
XLA Modules:
  0.0 135.4 jit_solution(8314999670824745449)
XLA Ops:
  0.0 1.0 fusion
  1.0 0.0 copy-start
  1.0 1.0 pad_maximum_fusion
  2.0 0.0 copy-done
  2.0 0.0 copy-start.1
  2.0 0.9 copy.14.refs_12_
  2.9 0.0 copy-done.1
  2.9 0.6 broadcast_in_dim.2.refs_1_
  3.5 130.0 %shard_map.127 = bf16[128,2048]{1,0:T(8,128)(2,1)} custom-call(bf16[128,2048]{1,0:T(8,128)(2,1)} %refs_0_.1, bf16[1,2048]{1,0:T(2,128)(2,1)} %broadcast_in_dim.2.refs_1_, bf16[512,256]{1,0:T(8,128)(2,1)} %refs_2_.1, bf16[512,256]{1,0:T(8,128)(2,1)} %refs_3_.1, bf16[512,256]{1,0:T(8,128)(2,1)} %refs_4_.1, bf16[512,256]{1,0:T(8,128)(2,1)} %refs_5_.1, ...), custom_call_target="tpu_custom_call" | custom-call | tf_op jit(solution)/shard_map/pallas_call | solution.py:571
  133.5 1.9 %copy.16 = bf16[128,2048]{1,0:T(8,128)(2,1)} copy(bf16[128,2048]{1,0:T(8,128)(2,1)} %shard_map.127) | data formatting | bytes 1048576
  (2 shorter events, 0.0 us)
Async XLA Ops:
  1.0 1.0 copy-start
  2.0 0.9 copy-start.1

commit v2 on v1

--- a/solution.py
+++ b/solution.py
@@ -1,4 +1,5 @@
 import functools
+import math
 
 import jax
 import jax.numpy as jnp
@@ -186,9 +187,8 @@
 
 MESH = pl.DeviceIdType.MESH
 NPROJ = 7
-LAG = 2
-ORDER = (3, 4, 5, 6, 0, 1, 2)
-QUERY, KEY, VALUE, GATE, OUTER, INNER, INPUT = range(NPROJ)
+ORDER = (3, 4, 5, 6, 1, 2, 0)
+QUERY, KEY, VALUE, GATE, INNER, INPUT, OUTER = range(NPROJ)
 
 
 def remote(src, dst, send, recv, axis, to):
@@ -199,9 +199,9 @@
 
 def kernel(sizes, *refs):
     n, g, m = sizes
-    tokens, gain, w0, w1, w2, w3, w4, w5, w6, taps, oc, orr, ld, ldt, cos2, sin2, out = refs[:17]
-    (raw, xn, gw, go, acc, ext, qr, kr, cum_s, cumt_s, lend, dec, instate, indec, sin_s, rb, cb, stage, land, tail, own) = refs[17:38]
-    (tsend, trecv, rsend, lsend, zrecv, ysend, yrecv, ssend, srecv, dsend, drecv, csend, crecv, osend, orecv) = refs[38:]
+    tokens, gain, w0, w1, w2, w3, w4, w5, w6, taps, oc, orr, ldt, out = refs[:14]
+    (raw, xn, gw, go, acc, ext, qr, kr, cum_s, cumt_s, cos2, sin2, kept_s, conv_s, lend, dec, instate, indec, sin_s, rb, cb, tail, own, swap) = refs[14:38]
+    (tsend, trecv, rsend, lsend, zrecv, ysend, yrecv, ssend, srecv, dsend, drecv, csend, crecv, osend, orecv, xsend, xrecv, bsend, brecv, fsend, frecv) = refs[38:]
     weights = [(w0, w1, w2, w3, w4, w5, w6)[i] for i in ORDER]
     outs = (oc, orr)
     me = lax.axis_index("sp")
@@ -223,18 +223,22 @@
             pl.semaphore_signal(barrier, inc=1, device_id={axis: lax.rem(at + d, count)}, device_id_type=MESH)
     pl.semaphore_wait(barrier, n + g + m - 3)
 
-    def token_copy(d):
-        to = lax.rem(mine + d, m)
-        return remote(tokens, raw.at[d - 1], tsend.at[d - 1], trecv.at[d - 1], "tp", to)
-
-    for d in range(1, m):
-        token_copy(d).start()
+    twin = mine + 1 - 2 * lax.rem(mine, 2)
+    far = lax.rem(mine + 2, m)
+    far_twin = far + 1 - 2 * lax.rem(far, 2)
+
+    def token_copy(k):
+        src = raw.at[1] if k == 2 else tokens
+        return remote(src, raw.at[k], tsend.at[k], trecv.at[k], "tp", far if k == 1 else twin)
+
+    token_copy(1).start()
+    token_copy(0).start()
 
     hs = pl.ds(pl.multiple_of(grp * half, half), half)
     ohs = pl.ds(pl.multiple_of(grp * ohalf, ohalf), ohalf)
 
     def slot(w, s, is_out):
-        return go.at[w, s, ohs] if is_out else gw.at[w, s, hs]
+        return go.at[mine, w, s, ohs] if is_out else gw.at[w, s, hs]
 
     def sem_at(w, is_out):
         return w + NPROJ if is_out else w
@@ -263,13 +267,43 @@
         def _():
             line_copy(w, me, is_out, False, src).start()
 
+    def far_copy(w, s, src=None):
+        part = go.at[mine, w, s]
+        return remote(part if src is None else src, part, xsend.at[w, s], xrecv.at[w, s], "tp", far)
+
+    def twin_copy(w, s, src=None):
+        part = go.at[mine, w, s]
+        return remote(part if src is None else src, part, bsend.at[w, s], brecv.at[w, s], "tp", twin)
+
+    def relay_copy(w, s):
+        part = go.at[far, w, s]
+        return remote(part, part, fsend.at[w, s], frecv.at[w, s], "tp", twin)
+
+    for w in range(2):
+        far_copy(w, me, outs[w]).start()
+        twin_copy(w, me, outs[w]).start()
+
     below = lax.broadcasted_iota(jnp.int32, (total, total), 0) >= lax.broadcasted_iota(jnp.int32, (total, total), 1)
-    cum_s[...] = jnp.dot(below.astype(jnp.float32), ld[...], precision=HIGHEST_PRECISION, preferred_element_type=jnp.float32)
-    above = lax.broadcasted_iota(jnp.int32, (total, total), 0) <= lax.broadcasted_iota(jnp.int32, (total, total), 1)
-    cumt_s[...] = jnp.dot(ldt[...], above.astype(jnp.float32), precision=HIGHEST_PRECISION, preferred_element_type=jnp.float32)
+
+    def decay_sums():
+        lower = below.astype(jnp.float32)
+        nt = (((1,), (1,)), ((), ()))
+        cum_s[...] = lax.dot_general(lower, ldt[...], nt, precision=HIGHEST_PRECISION, preferred_element_type=jnp.float32)
+        cumt_s[...] = lax.dot_general(ldt[...], lower, nt, precision=HIGHEST_PRECISION, preferred_element_type=jnp.float32)
+
+    def tables():
+        half_width = HEAD // 2
+        lane = lax.broadcasted_iota(jnp.int32, (total, HEAD), 1)
+        first = lane < half_width
+        index = jnp.where(first, lane, lane - half_width).astype(jnp.float32)
+        place = (lax.broadcasted_iota(jnp.int32, (total, HEAD), 0) + me * total).astype(jnp.float32)
+        angle = place * jnp.exp(index * (-math.log(ROTARY_BASE) / half_width))
+        cos2[...] = jnp.cos(angle)
+        sine = jnp.sin(angle)
+        sin2[...] = jnp.where(first, -sine, sine)
 
     step_rows = 16
-    scale = gain[...].astype(jnp.float32)
+    scale = gain[...].astype(jnp.float32)[None, :]
 
     def normalise(source, block):
         def one(i, carry):
@@ -284,16 +318,6 @@
 
         lax.fori_loop(0, rows // step_rows, one, 0)
 
-    normalise(tokens, mine)
-    for d in range(1, m):
-        token_copy(d).wait_recv()
-        normalise(raw.at[d - 1], lax.rem(mine - d + m, m))
-
-    for w in range(NPROJ):
-        acc[w] = jnp.dot(xn[me], weights[w][...], preferred_element_type=jnp.float32)
-    for w in range(2):
-        go[w, me] = outs[w][...]
-
     def forward(w, is_out, d):
         @pl.when(me >= d)
         def _():
@@ -319,7 +343,7 @@
 
     def other_wait(w, s, is_out):
         theirs = (
-            go.at[w, s, pl.ds(pl.multiple_of(other * ohalf, ohalf), ohalf)]
+            go.at[mine, w, s, pl.ds(pl.multiple_of(other * ohalf, ohalf), ohalf)]
             if is_out
             else gw.at[w, s, pl.ds(pl.multiple_of(other * half, half), half)]
         )
@@ -339,26 +363,102 @@
             other_wait(w, s, False)
             acc[w] += jnp.dot(xn[s], gw[w, s], preferred_element_type=jnp.float32)
 
-    def phase(d, lo, hi):
+    def block_one():
+        token_copy(0).wait_recv()
+        normalise(raw.at[0], twin)
+
+    def block_two():
+        token_copy(1).wait_recv()
+        token_copy(2).start()
+        normalise(raw.at[1], far)
+
+    def block_three():
+        token_copy(2).wait_recv()
+        normalise(raw.at[2], far_twin)
+
+    def own_dots(which):
+        for w in which:
+            acc[w] = jnp.dot(xn[me], weights[w][...], preferred_element_type=jnp.float32)
+
+    def at_distance(d, act):
+        @pl.when(me >= d)
+        def _():
+            act(me - d)
+
+        @pl.when(me + d < n)
+        def _():
+            act(me + d)
+
+    def share(d):
+        def act(s):
+            for w in range(2):
+                other_wait(w, s, True)
+                far_copy(w, s).start()
+                twin_copy(w, s).start()
+
+        at_distance(d, act)
+
+    def relay(d):
+        def act(s):
+            for w in range(2):
+                far_copy(w, s).wait_recv()
+                relay_copy(w, s).start()
+
+        at_distance(d, act)
+
+    def keep_own():
+        for w in range(2):
+            go[mine, w, me] = outs[w][...]
+
+    def relay_own():
+        for w in range(2):
+            far_copy(w, me).wait_recv()
+            relay_copy(w, me).start()
+
+    def own_low():
+        own_dots(range(4))
+
+    def own_high():
+        own_dots(range(4, NPROJ))
+
+    jobs = [decay_sums, tables, lambda: normalise(tokens, mine), block_one, block_two, block_three, own_low, own_high, keep_own]
+    forward(0, True, 1)
+    jobs[0]()
+    forward(1, True, 1)
+    jobs[1]()
+    for w in range(NPROJ):
+        forward(w, False, 1)
+        jobs[w + 2]()
+    share(1)
+    relay_own()
+
+    def steps(d, lo, hi):
         def one(i, carry):
-            @pl.when(i < hi)
-            def _():
-                forward(i, False, d)
-
-            @pl.when(i >= lo + LAG)
-            def _():
-                consume(i - LAG, d)
-
+            forward(i, False, d)
+            consume(i, d - 1)
             return carry
 
-        lax.fori_loop(lo, hi + LAG, one, 0)
-
-    for d in range(1, n):
+        lax.fori_loop(lo, hi, one, 0)
+
+    def finish(lo, hi):
+        if n < 3:
+            return
+
+        def one(i, carry):
+            consume(i, n - 1)
+            return carry
+
+        lax.fori_loop(lo, hi, one, 0)
+
+    for d in range(2, n):
         forward(0, True, d)
         forward(1, True, d)
+        steps(d, 0, 3)
+        share(d)
+        relay(d - 1)
         if d < n - 1:
-            phase(d, 0, NPROJ)
-    phase(n - 1, 0, 3)
+            steps(d, 3, NPROJ)
+    finish(0, 3)
 
     def projected(w, h=None):
         part = acc[w] if h is None else acc[w, :, h * HEAD : (h + 1) * HEAD]
@@ -390,40 +490,84 @@
             state_copy(d).start()
             decay_copy(d).start()
 
-    phase(n - 1, 3, NPROJ)
-
-    mixed_in = projected(INNER) * projected(INPUT)
-    ext[8:, :] = mixed_in
-    tail[...] = mixed_in[total - 8 :, :]
-
-    def rim_copy():
-        return remote(tail, ext.at[0:8], csend, crecv, "sp", me + 1)
-
-    @pl.when(me < n - 1)
-    def _():
-        rim_copy().start()
-
-    sin_s[...] = jnp.zeros_like(sin_s)
-    for s in range(n - 1):
-
-        @pl.when(me > s)
-        def _():
-            remote(lend, instate.at[s], ssend.at[0], srecv.at[s], "sp", s).wait_recv()
-            remote(dec, indec.at[s], dsend.at[0], drecv.at[s], "sp", s).wait_recv()
-            for h in range(heads):
-                sin_s[h] = jnp.exp(indec[s, h : h + 1, :]) * sin_s[h] + instate[s, h].astype(jnp.float32)
-
+    values = [acc[VALUE, :, h * HEAD : (h + 1) * HEAD].astype(jnp.bfloat16) for h in range(heads)]
+    steps(n - 1, 3, 4)
     for h in range(heads):
         c = cum_s[:, h : h + 1]
         spread = c - cumt_s[h : h + 1, :]
         grid = jnp.where(below, jnp.exp(jnp.where(below, spread, 0.0)), 0.0)
         scores = lax.dot_general(qr[h], kr[h], (((1,), (1,)), ((), ())), preferred_element_type=jnp.float32) * grid
-        vals = acc[VALUE, :, h * HEAD : (h + 1) * HEAD].astype(jnp.bfloat16)
-        kept = jnp.dot(scores.astype(jnp.bfloat16), vals, preferred_element_type=jnp.float32)
+        kept_s[h] = jnp.dot(scores.astype(jnp.bfloat16), values[h], preferred_element_type=jnp.float32)
+        steps(n - 1, 4 + h, 5 + h) if h < 2 else None
+    steps(n - 1, min(4 + heads, 6), NPROJ)
+    relay(n - 1)
+    finish(3, 4)
+
+    sin_s[...] = jnp.zeros_like(sin_s)
+    for s in range(n - 1):
+
+        @pl.when(me > s)
+        def _():
+            remote(lend, instate.at[s], ssend.at[0], srecv.at[s], "sp", s).wait_recv()
+            remote(dec, indec.at[s], dsend.at[0], drecv.at[s], "sp", s).wait_recv()
+            for h in range(heads):
+                sin_s[h] = jnp.exp(indec[s, h : h + 1, :]) * sin_s[h] + instate[s, h].astype(jnp.float32)
+
+    for h in range(heads):
+        c = cum_s[:, h : h + 1]
+        kept = kept_s[h]
         kept += jnp.dot(qr[h], sin_s[h].astype(jnp.bfloat16), preferred_element_type=jnp.float32) * jnp.exp(c)
         gate = projected(GATE, h)
         normed = kept * lax.rsqrt(jnp.mean(kept * kept, axis=-1, keepdims=True) + EPSILON)
         rb[:, h * HEAD : (h + 1) * HEAD] = (normed * (gate / (1.0 + jnp.exp(-gate)))).astype(jnp.bfloat16)
+
+    def block(ref, to):
+        return ref.at[pl.ds(pl.multiple_of(to * rows, rows), rows)]
+
+    def branch_copy(kind, k):
+        to = (twin, far, far_twin)[k]
+        return remote(block((cb, rb)[kind], to), swap.at[kind, k], osend.at[kind, k], orecv.at[kind, k], "tp", to)
+
+    for k in (1, 2, 0):
+        branch_copy(1, k).start()
+
+    finish(INNER, INPUT + 1)
+    mixed_in = projected(INNER) * projected(INPUT)
+    ext[8:, :] = mixed_in
+    tail[...] = mixed_in[total - 8 :, :]
+
+    def rim_copy():
+        return remote(tail, ext.at[0:8], csend, crecv, "sp", me + 1)
+
+    @pl.when(me < n - 1)
+    def _():
+        rim_copy().start()
+
+    for d in range(1, n):
+        at_distance(d, lambda s: [twin_copy(w, s).wait_recv() for w in range(2)])
+        at_distance(d, lambda s: [relay_copy(w, s).wait_recv() for w in range(2)])
+    for w in range(2):
+        twin_copy(w, me).wait_recv()
+        relay_copy(w, me).wait_recv()
+
+    owners = (twin, far, far_twin)
+
+    def add_branch(kind):
+        at = pl.ds(pl.multiple_of(mine * rows, rows), rows)
+        for k in range(m - 1):
+            branch_copy(kind, k).wait_recv()
+        parts = [(cb, rb)[kind][at, :]] + [swap[kind, k] for k in range(m - 1)]
+        for s in range(n):
+            to = slice(s * ocols, (s + 1) * ocols)
+            value = jnp.dot(parts[0], go[mine, kind, s], preferred_element_type=jnp.float32)
+            for k in range(m - 1):
+                value += jnp.dot(parts[k + 1], go[owners[k], kind, s], preferred_element_type=jnp.float32)
+            if kind == 1:
+                own[:, to] = value
+            else:
+                out[:, to] = (own[:, to] + value).astype(jnp.bfloat16)
+
+    add_branch(1)
 
     @pl.when(me > 0)
     def _():
@@ -438,47 +582,22 @@
     for j in range(CONV_K):
         lo = 8 - (CONV_K - 1) + j
         conv = conv + t[j : j + 1, :] * ext[lo : lo + total, :]
-    cb[...] = (projected(OUTER) * conv).astype(jnp.bfloat16)
-
-    for d in range(1, n):
-        for w in range(2):
-
-            @pl.when(me >= d)
-            def _():
-                other_wait(w, me - d, True)
-
-            @pl.when(me + d < n)
-            def _():
-                other_wait(w, me + d, True)
-
-    def partial(block, s):
-        at = pl.ds(pl.multiple_of(block * rows, rows), rows)
-        return jnp.dot(cb[at, :], go[0, s], preferred_element_type=jnp.float32) + jnp.dot(
-            rb[at, :], go[1, s], preferred_element_type=jnp.float32
-        )
-
-    def out_copy(d):
-        return remote(stage.at[d - 1], land.at[d - 1], osend.at[d - 1], orecv.at[d - 1], "tp", lax.rem(mine + d, m))
-
-    for d in range(1, m):
-        block = lax.rem(mine + d, m)
+    conv_s[...] = conv
+    finish(OUTER, OUTER + 1)
+    cb[...] = (projected(OUTER) * conv_s[...]).astype(jnp.bfloat16)
+    for k in (1, 2, 0):
+        branch_copy(0, k).start()
+    add_branch(0)
+
+    for k in range(m - 1):
+        token_copy(k).wait_send()
+        for kind in range(2):
+            branch_copy(kind, k).wait_send()
+    for w in range(2):
         for s in range(n):
-            stage[d - 1, :, s * ocols : (s + 1) * ocols] = partial(block, s).astype(jnp.bfloat16)
-        out_copy(d).start()
-    for s in range(n):
-        own[:, s * ocols : (s + 1) * ocols] = partial(mine, s)
-    for d in range(1, m):
-        out_copy(d).wait_recv()
-    for s in range(n):
-        at = slice(s * ocols, (s + 1) * ocols)
-        value = own[:, at].astype(jnp.bfloat16).astype(jnp.float32)
-        for d in range(1, m):
-            value = value + land[d - 1, :, at].astype(jnp.float32)
-        out[:, at] = value.astype(jnp.bfloat16)
-
-    for d in range(1, m):
-        token_copy(d).wait_send()
-        out_copy(d).wait_send()
+            far_copy(w, s).wait_send()
+            twin_copy(w, s).wait_send()
+            relay_copy(w, s).wait_send()
     for d in range(1, n):
 
         @pl.when(me + d < n)
@@ -521,26 +640,23 @@
     orows, ocols = args[10].shape
     total = rows * m
     heads = cols // HEAD
-    half_width = HEAD // 2
-    inv_freq = ROTARY_BASE ** (-jnp.arange(half_width, dtype=jnp.float32) / half_width)
-    offset = (lax.axis_index("sp") * total).astype(jnp.float32)
-    angles = (offset + jnp.arange(total, dtype=jnp.float32))[:, None] * inv_freq[None, :]
-    cosine, sine = jnp.cos(angles), jnp.sin(angles)
-    cos2 = jnp.concatenate([cosine, cosine], axis=1)
-    sin2 = jnp.concatenate([-sine, sine], axis=1)
     bf, f32 = jnp.bfloat16, jnp.float32
     dma = pltpu.SemaphoreType.DMA
     scratch = [
         pltpu.VMEM((m - 1, rows, width), bf),
         pltpu.VMEM((n, total, depth), bf),
         pltpu.VMEM((NPROJ, n, depth, cols), bf),
-        pltpu.VMEM((2, n, orows, ocols), bf),
+        pltpu.VMEM((m, 2, n, orows, ocols), bf),
         pltpu.VMEM((NPROJ, total, cols), f32),
         pltpu.VMEM((total + 8, cols), f32),
         pltpu.VMEM((heads, total, HEAD), bf),
         pltpu.VMEM((heads, total, HEAD), bf),
         pltpu.VMEM((total, heads), f32),
         pltpu.VMEM((heads, total), f32),
+        pltpu.VMEM((total, HEAD), f32),
+        pltpu.VMEM((total, HEAD), f32),
+        pltpu.VMEM((heads, total, HEAD), f32),
+        pltpu.VMEM((total, cols), f32),
         pltpu.VMEM((heads, HEAD, HEAD), bf),
         pltpu.VMEM((8, HEAD), f32),
         pltpu.VMEM((n, heads, HEAD, HEAD), bf),
@@ -548,10 +664,9 @@
         pltpu.VMEM((heads, HEAD, HEAD), f32),
         pltpu.VMEM((total, cols), bf),
         pltpu.VMEM((total, cols), bf),
-        pltpu.VMEM((m - 1, rows, width), bf),
-        pltpu.VMEM((m - 1, rows, width), bf),
         pltpu.VMEM((8, cols), f32),
         pltpu.VMEM((rows, width), f32),
+        pltpu.VMEM((2, m - 1, rows, cols), bf),
         dma((m - 1,)),
         dma((m - 1,)),
         dma((NPROJ + 2, n)),
@@ -565,19 +680,19 @@
         dma((n,)),
         dma,
         dma,
-        dma((m - 1,)),
-        dma((m - 1,)),
-    ]
+        dma((2, m - 1)),
+        dma((2, m - 1)),
+    ] + [dma((2, n))] * 6
     return pl.pallas_call(
         functools.partial(kernel, sizes),
         out_shape=jax.ShapeDtypeStruct((rows, width), bf),
-        in_specs=[pl.BlockSpec(memory_space=pltpu.VMEM)] * 16,
+        in_specs=[pl.BlockSpec(memory_space=pltpu.VMEM)] * 13,
         out_specs=pl.BlockSpec(memory_space=pltpu.VMEM),
         scratch_shapes=scratch,
         compiler_params=pltpu.CompilerParams(
             collective_id=0, has_side_effects=True, vmem_limit_bytes=60 * 1024 * 1024
         ),
-    )(tokens, gain[None, :], *args[2:12], log_decay, log_decay.T, cos2, sin2)
+    )(tokens, gain, *args[2:12], log_decay.T)
 
 
 def solution(mesh):
@@ -597,7 +712,7 @@
         P(("grp", "sp"), "tp"),
     )
     n, g, m = (mesh.shape[axis] for axis in ("sp", "grp", "tp"))
-    fits = g == 2 and 2 <= n <= 4
+    fits = g == 2 and m == 4 and 3 <= n <= 4
     return jax.shard_map(
         functools.partial(fused, (n, g, m)) if fits else body, mesh=mesh, in_specs=placed, out_specs=P(("grp", "sp", "tp"), None), check_vma=False
     )

time: 136 us -> 103 us (0.76)
  Pallas kernels: 130 us -> 101 us
  other arithmetic: 2 us -> 0 us
  local copies, waits for them, and re-layouts: 3.36 us -> 1.88 us
    pallas_call x1, Pallas kernels: 130 us -> 101 us  [fused(): pl.pallas_call(functools.partial(kernel, sizes), out_shape=jax.ShapeDtype...]
    unnamed x6 -> x1, local copies, waits for them, and re-layouts: 2.75 us -> 1.88 us
where the time goes in v2:
time: 103 us
  Pallas kernels  101 us (98%)
  local copies, waits for them, and re-layouts  1.88 us (2%)
    pallas_call x1, Pallas kernels, fused(): pl.pallas_call(functools.partial(kernel, sizes), out_shape=jax.ShapeDtype...  101 us

profile of v2, /device:TPU:11, one launch (start us, length us, event | category | flops | bytes accessed | tf_op | source)
XLA Modules:
  0.0 102.6 jit_solution(12533506700042074634)
XLA Ops:
  0.0 100.7 %shard_map.127 = bf16[128,2048]{1,0:T(8,128)(2,1)} custom-call(bf16[128,2048]{1,0:T(8,128)(2,1)} %refs_0_.1, bf16[2048]{0:T(1024)(128)(2,1)} %refs_1_.1, bf16[512,256]{1,0:T(8,128)(2,1)} %refs_2_.1, bf16[512,256]{1,0:T(8,128)(2,1)} %refs_3_.1, bf16[512,256]{1,0:T(8,128)(2,1)} %refs_4_.1, bf16[512,256]{1,0:T(8,128)(2,1)} %refs_5_.1, ...), custom_call_target="tpu_custom_call" | custom-call | tf_op jit(solution)/shard_map/pallas_call | solution.py:686
  100.7 1.9 %copy.15 = bf16[128,2048]{1,0:T(8,128)(2,1)} copy(bf16[128,2048]{1,0:T(8,128)(2,1)} %shard_map.127) | data formatting | bytes 1048576

commit v3 on v2

--- a/solution.py
+++ b/solution.py
@@ -291,16 +291,21 @@
         cum_s[...] = lax.dot_general(lower, ldt[...], nt, precision=HIGHEST_PRECISION, preferred_element_type=jnp.float32)
         cumt_s[...] = lax.dot_general(ldt[...], lower, nt, precision=HIGHEST_PRECISION, preferred_element_type=jnp.float32)
 
-    def tables():
+    pieces = NPROJ + 1
+    piece_rows = total // pieces
+
+    def tables(i):
         half_width = HEAD // 2
-        lane = lax.broadcasted_iota(jnp.int32, (total, HEAD), 1)
+        lane = lax.broadcasted_iota(jnp.int32, (piece_rows, HEAD), 1)
         first = lane < half_width
         index = jnp.where(first, lane, lane - half_width).astype(jnp.float32)
-        place = (lax.broadcasted_iota(jnp.int32, (total, HEAD), 0) + me * total).astype(jnp.float32)
+        start = i * piece_rows
+        place = (lax.broadcasted_iota(jnp.int32, (piece_rows, HEAD), 0) + me * total + start).astype(jnp.float32)
         angle = place * jnp.exp(index * (-math.log(ROTARY_BASE) / half_width))
-        cos2[...] = jnp.cos(angle)
+        at = pl.ds(start if isinstance(start, int) else pl.multiple_of(start, piece_rows), piece_rows)
+        cos2[at, :] = jnp.cos(angle)
         sine = jnp.sin(angle)
-        sin2[...] = jnp.where(first, -sine, sine)
+        sin2[at, :] = jnp.where(first, -sine, sine)
 
     step_rows = 16
     scale = gain[...].astype(jnp.float32)[None, :]
@@ -421,21 +426,23 @@
     def own_high():
         own_dots(range(4, NPROJ))
 
-    jobs = [decay_sums, tables, lambda: normalise(tokens, mine), block_one, block_two, block_three, own_low, own_high, keep_own]
+    jobs = [lambda: normalise(tokens, mine), block_one, block_two, block_three, own_low, own_high, keep_own]
+    decay_sums()
     forward(0, True, 1)
-    jobs[0]()
     forward(1, True, 1)
-    jobs[1]()
     for w in range(NPROJ):
         forward(w, False, 1)
-        jobs[w + 2]()
+        jobs[w]()
     share(1)
     relay_own()
+    tables(NPROJ)
 
     def steps(d, lo, hi):
         def one(i, carry):
             forward(i, False, d)
             consume(i, d - 1)
+            if d == 2:
+                tables(i)
             return carry
 
         lax.fori_loop(lo, hi, one, 0)
@@ -458,6 +465,7 @@
         relay(d - 1)
         if d < n - 1:
             steps(d, 3, NPROJ)
+    steps(n - 1, 3, 4)
     finish(0, 3)
 
     def projected(w, h=None):
@@ -483,6 +491,8 @@
         vals = acc[VALUE, :, h * HEAD : (h + 1) * HEAD].astype(jnp.bfloat16)
         lend[h] = lax.dot_general(kw, vals, (((0,), (0,)), ((), ())), preferred_element_type=jnp.float32).astype(jnp.bfloat16)
         dec[h : h + 1, :] = jnp.broadcast_to(end, (1, HEAD))
+        if h == 0:
+            steps(n - 1, 4, 5)
     for d in range(1, n):
 
         @pl.when(me + d < n)
@@ -491,15 +501,15 @@
             decay_copy(d).start()
 
     values = [acc[VALUE, :, h * HEAD : (h + 1) * HEAD].astype(jnp.bfloat16) for h in range(heads)]
-    steps(n - 1, 3, 4)
+    steps(n - 1, 5, 6)
     for h in range(heads):
         c = cum_s[:, h : h + 1]
         spread = c - cumt_s[h : h + 1, :]
         grid = jnp.where(below, jnp.exp(jnp.where(below, spread, 0.0)), 0.0)
         scores = lax.dot_general(qr[h], kr[h], (((1,), (1,)), ((), ())), preferred_element_type=jnp.float32) * grid
         kept_s[h] = jnp.dot(scores.astype(jnp.bfloat16), values[h], preferred_element_type=jnp.float32)
-        steps(n - 1, 4 + h, 5 + h) if h < 2 else None
-    steps(n - 1, min(4 + heads, 6), NPROJ)
+        if h == 0:
+            steps(n - 1, 6, NPROJ)
     relay(n - 1)
     finish(3, 4)
 
@@ -712,7 +722,7 @@
         P(("grp", "sp"), "tp"),
     )
     n, g, m = (mesh.shape[axis] for axis in ("sp", "grp", "tp"))
-    fits = g == 2 and m == 4 and 3 <= n <= 4
+    fits = g == 2 and m == 4 and n == 4
     return jax.shard_map(
         functools.partial(fused, (n, g, m)) if fits else body, mesh=mesh, in_specs=placed, out_specs=P(("grp", "sp", "tp"), None), check_vma=False
     )

time: 103 us -> 104 us (level)
  no operation moved by 1% of the time
where the time goes in v3:
time: 104 us; the launch traced here: 103 us
  Pallas kernels  101 us (97%)
  local copies, waits for them, and re-layouts  1.88 us (2%)
    pallas_call x1, Pallas kernels, fused(): pl.pallas_call(functools.partial(kernel, sizes), out_shape=jax.ShapeDtype...  101 us

profile of v3, /device:TPU:11, one launch (start us, length us, event | category | flops | bytes accessed | tf_op | source)
XLA Modules:
  0.0 103.1 jit_solution(7513857525436745200)
XLA Ops:
  0.0 101.3 %shard_map.127 = bf16[128,2048]{1,0:T(8,128)(2,1)} custom-call(bf16[128,2048]{1,0:T(8,128)(2,1)} %refs_0_.1, bf16[2048]{0:T(1024)(128)(2,1)} %refs_1_.1, bf16[512,256]{1,0:T(8,128)(2,1)} %refs_2_.1, bf16[512,256]{1,0:T(8,128)(2,1)} %refs_3_.1, bf16[512,256]{1,0:T(8,128)(2,1)} %refs_4_.1, bf16[512,256]{1,0:T(8,128)(2,1)} %refs_5_.1, ...), custom_call_target="tpu_custom_call" | custom-call | tf_op jit(solution)/shard_map/pallas_call | solution.py:696
  101.3 1.9 %copy.15 = bf16[128,2048]{1,0:T(8,128)(2,1)} copy(bf16[128,2048]{1,0:T(8,128)(2,1)} %shard_map.127) | data formatting | bytes 1048576
